TPU v7x, 32 devices: a whole 2x2x4 slice. The times are simulated.
32 devices in a mesh: ep: 8 (over z, y), tp: 4 (over x, core).
Axes of the slice: x: 2, y: 2, z: 4, core: 2. Of those that a mesh axis runs over, the one named last changes fastest.
Arguments:
- queries: bfloat16 [2048, 1536], P('ep', 'tp'), may hold values from -6 to 6
- kv_latent: bfloat16 [2048, 512], P('ep'), may hold values from -6 to 6
- rope_key: bfloat16 [2048, 64], P('ep'), may hold values from -6 to 6
- latent_gain: float32 [512], replicated, may hold values from 0.1 to 1.9
- w_key_up: bfloat16 [512, 1024], P(None, 'tp'), may hold values from -0.25 to 0.25
- w_value_up: bfloat16 [512, 1024], P(None, 'tp'), may hold values from -0.25 to 0.25
- query_gain: float32 [192], replicated, may hold values from 0.1 to 1.9
- key_gain: float32 [128], replicated, may hold values from 0.1 to 1.9
- rope_gain: float32 [64], replicated, may hold values from 0.1 to 1.9
- out_gain: float32 [128], replicated, may hold values from 0.1 to 1.9
- moe_tokens: bfloat16 [2048, 2048], P('ep'), may hold values from -6 to 6
- moe_gain: float32 [2048], replicated, may hold values from 0.1 to 1.9
- routes: int32 [2048, 2], P('ep'), may hold values from 0 to 7, all different within a row; in each aligned block of 64 rows (0 to 63, 64 to 127, ...) at most 24 rows name the same one
- route_weights: float32 [2048, 2], P('ep'), may hold values from 0.25 to 1
- w_gate: bfloat16 [8, 2048, 3584], P('ep', None, 'tp'), may hold values from -0.125 to 0.125
- w_up: bfloat16 [8, 2048, 3584], P('ep', None, 'tp'), may hold values from -0.125 to 0.125
- w_down: bfloat16 [8, 3584, 2048], P('ep', 'tp'), may hold values from -0.09375 to 0.09375
Outputs:
- attended: bfloat16 [2048, 1024], P('ep', 'tp')
- moe_out: bfloat16 [2048, 2048], P(('ep', 'tp'))
Inputs may be any that keep to these rules, and one draw needn't show every extreme that they name: `routes`: each row names 2 different experts of 0 to 7; in each aligned block of 64 rows no expert is named by more than 24 rows, and in some block one expert is named by exactly 24.
All inputs are finite; a program needn't handle non-finite values.
Results may differ from a plain program's by a relative error of at most 0.0071.
Values may be sent and summed in bfloat16 or wider, within the bound.
A program may use at most 128 MiB of HBM per device.

v0:
```python
import math
import jax
import jax.numpy as jnp
from jax import lax
from jax.sharding import PartitionSpec as P

EPS = 1e-06
THETA = 500000.0


def rms_norm(values, norm_gain):
    return values * lax.rsqrt(jnp.mean(values * values, axis=-1, keepdims=True) + EPS) * norm_gain


def rope_tables(positions, rope_dim):
    freqs = 1.0 / THETA ** (jnp.arange(0, rope_dim, 2, dtype=jnp.float32) / rope_dim)
    angles = positions.astype(jnp.float32)[:, None] * freqs[None, :]
    return (jnp.cos(angles), jnp.sin(angles))


def rotate(values, rot_cos, rot_sin):
    half_dim = values.shape[-1] // 2
    first_half = values[..., :half_dim]
    second_half = values[..., half_dim:]
    return jnp.concatenate(
        [
            first_half * rot_cos - second_half * rot_sin,
            second_half * rot_cos + first_half * rot_sin,
        ],
        axis=-1,
    )


def attention_part(
    queries,
    kv_latent,
    rope_key,
    latent_gain,
    w_key_up,
    w_value_up,
    query_gain,
    key_gain,
    rope_gain,
    out_gain,
):
    tok_rows = queries.shape[0]
    nope_dim = key_gain.shape[0]
    value_dim = out_gain.shape[0]
    rope_dim = rope_key.shape[1]
    head_count = w_key_up.shape[1] // nope_dim
    offset = lax.axis_index("ep") * tok_rows
    positions = offset + jnp.arange(tok_rows, dtype=jnp.int32)
    rot_cos, rot_sin = rope_tables(positions, rope_dim)
    latent = rms_norm(kv_latent.astype(jnp.float32), latent_gain).astype(jnp.bfloat16)
    key_nope = jnp.dot(latent, w_key_up, preferred_element_type=jnp.float32).reshape(
        tok_rows, head_count, nope_dim
    )
    key_nope = (
        rms_norm(key_nope, key_gain).astype(jnp.bfloat16).reshape(tok_rows, head_count * nope_dim)
    )
    values = jnp.dot(latent, w_value_up, preferred_element_type=jnp.float32).astype(jnp.bfloat16)
    rot_key = rotate(rms_norm(rope_key.astype(jnp.float32), rope_gain), rot_cos, rot_sin).astype(
        jnp.bfloat16
    )
    keys_values = jnp.concatenate([key_nope, values], axis=1)
    query = rms_norm(
        queries.astype(jnp.float32).reshape(tok_rows, head_count, nope_dim + rope_dim), query_gain
    )
    query_nope = query[..., :nope_dim].astype(jnp.bfloat16)
    query_rope = rotate(query[..., nope_dim:], rot_cos[:, None, :], rot_sin[:, None, :]).astype(
        jnp.bfloat16
    )
    scale = (nope_dim + rope_dim) ** (-0.5)
    last_pos = offset + tok_rows - 1
    initial = (
        jnp.zeros((tok_rows, head_count, value_dim), jnp.float32),
        jnp.zeros((head_count, tok_rows), jnp.float32),
    )
    totals = initial
    key_piece = lax.all_gather(keys_values, "ep", axis=0, tiled=True)
    rope_piece = lax.all_gather(rot_key, "ep", axis=0, tiled=True)
    piece_rows = key_piece.shape[0]
    block_rows = math.gcd(piece_rows, 512)

    def one_block(totals_in, block_index):
        block_first = block_index * block_rows
        kv_block = lax.dynamic_slice_in_dim(key_piece, block_first, block_rows, 0)
        rope_block = lax.dynamic_slice_in_dim(rope_piece, block_first, block_rows, 0)

        def attend(sums_in):
            weighted, denominator = sums_in
            key_block = kv_block[:, : head_count * nope_dim].reshape(
                block_rows, head_count, nope_dim
            )
            value_block = kv_block[:, head_count * nope_dim :].reshape(
                block_rows, head_count, value_dim
            )
            scores = (
                jnp.einsum(
                    "qhd,khd->hqk", query_nope, key_block, preferred_element_type=jnp.float32
                )
                + jnp.einsum(
                    "qhr,kr->hqk", query_rope, rope_block, preferred_element_type=jnp.float32
                )
            ) * scale
            key_pos = block_first + jnp.arange(block_rows, dtype=jnp.int32)
            visible = (positions[:, None] >= key_pos[None, :])[None]
            exp_scores = jnp.where(visible, jnp.exp(scores), 0.0)
            denominator = denominator + jnp.sum(exp_scores, axis=-1)
            weighted = weighted + jnp.einsum(
                "hqk,khd->qhd",
                exp_scores.astype(jnp.bfloat16),
                value_block,
                preferred_element_type=jnp.float32,
            )
            return (weighted, denominator)

        def unchanged(sums_in):
            return sums_in

        return (lax.cond(block_first <= last_pos, attend, unchanged, totals_in), None)

    totals, _ = lax.scan(one_block, totals, jnp.arange(piece_rows // block_rows, dtype=jnp.int32))
    weighted, denominator = totals
    mixed = weighted / jnp.transpose(denominator)[:, :, None]
    return rms_norm(mixed, out_gain).astype(jnp.bfloat16).reshape(tok_rows, head_count * value_dim)


def experts_part(moe_tokens, moe_gain, routes, route_weights, w_gate, w_up, w_down):
    n_rows = moe_tokens.shape[0]
    model_dim = moe_tokens.shape[1]
    top_count = routes.shape[1]
    quarters = lax.axis_size("tp")
    part_rows = n_rows // quarters
    experts = lax.axis_size("ep") * w_gate.shape[0]
    capacity = (3 * top_count * part_rows + 2 * experts - 1) // (2 * experts)
    slot_count = experts * capacity
    normed = rms_norm(moe_tokens.astype(jnp.float32), moe_gain).astype(jnp.bfloat16)
    chosen = routes.reshape(quarters, part_rows * top_count)
    onehot = (chosen[..., None] == jnp.arange(experts, dtype=jnp.int32)).astype(jnp.int32)
    rank = jnp.sum((jnp.cumsum(onehot, axis=1) - onehot) * onehot, axis=-1)
    slots = chosen * capacity + rank
    slot_hit = (slots[..., None] == jnp.arange(slot_count, dtype=jnp.int32)).astype(jnp.bfloat16)
    slot_hit = slot_hit.reshape(quarters, part_rows, top_count, slot_count)
    my_part = lax.axis_index("tp")
    mine_hit = lax.dynamic_index_in_dim(slot_hit, my_part, 0, keepdims=False)
    down_cols = w_down[0]
    own_rows = lax.dynamic_slice_in_dim(normed, my_part * part_rows, part_rows, 0)
    outgoing = jnp.einsum(
        "rs,rd->sd", jnp.sum(mine_hit, axis=1), own_rows, preferred_element_type=jnp.float32
    )
    outgoing = outgoing.astype(jnp.bfloat16).reshape(1, experts, capacity, model_dim)
    arrived = lax.all_gather(
        lax.all_to_all(outgoing, "ep", split_axis=1, concat_axis=1, tiled=True),
        "tp",
        axis=0,
        tiled=True,
    )
    gate = jnp.einsum("abcd,df->abcf", arrived, w_gate[0], preferred_element_type=jnp.float32)
    upward = jnp.einsum("abcd,df->abcf", arrived, w_up[0], preferred_element_type=jnp.float32)
    hidden = (jax.nn.silu(gate) * upward).astype(jnp.bfloat16)
    summed = lax.psum_scatter(
        jnp.einsum("abcf,fd->abcd", hidden, down_cols, preferred_element_type=jnp.float32),
        "tp",
        scatter_dimension=0,
        tiled=True,
    ).astype(jnp.bfloat16)
    returned = lax.all_to_all(summed, "ep", split_axis=1, concat_axis=1, tiled=True)
    picked = jnp.einsum(
        "rks,sd->rkd",
        mine_hit,
        returned.reshape(slot_count, model_dim),
        preferred_element_type=jnp.float32,
    )
    own_weights = lax.dynamic_slice_in_dim(route_weights, my_part * part_rows, part_rows, 0)
    return jnp.sum(picked * own_weights[:, :, None], axis=1).astype(jnp.bfloat16)


def on_device(
    queries,
    kv_latent,
    rope_key,
    latent_gain,
    w_key_up,
    w_value_up,
    query_gain,
    key_gain,
    rope_gain,
    out_gain,
    moe_tokens,
    moe_gain,
    routes,
    route_weights,
    w_gate,
    w_up,
    w_down,
):
    attended = attention_part(
        queries,
        kv_latent,
        rope_key,
        latent_gain,
        w_key_up,
        w_value_up,
        query_gain,
        key_gain,
        rope_gain,
        out_gain,
    )
    moe_out = experts_part(moe_tokens, moe_gain, routes, route_weights, w_gate, w_up, w_down)
    return (attended, moe_out)


def solution(mesh):
    return jax.shard_map(
        on_device,
        mesh=mesh,
        in_specs=(
            P("ep", "tp"),
            P("ep", None),
            P("ep", None),
            P(),
            P(None, "tp"),
            P(None, "tp"),
            P(),
            P(),
            P(),
            P(),
            P("ep", None),
            P(),
            P("ep", None),
            P("ep", None),
            P("ep", None, "tp"),
            P("ep", None, "tp"),
            P("ep", "tp", None),
        ),
        out_specs=(P("ep", "tp"), P(("ep", "tp"), None)),
        check_vma=False,
    )
```

profile of v0, /device:TPU:24, one launch (start us, length us, event | category | flops | bytes accessed | tf_op | source)
XLA Modules:
  0.0 215.2 jit_solution(17338202645033800728)
XLA Ops:
  8.1 0.8 copy.48
  9.6 1.5 multiply_reduce_fusion
  11.1 1.5 convert_element_type.75
  14.4 23.4 %all_to_all.10 = bf16[1,8,24,2048]{3,2,0,1:T(8,128)(2,1)} all-to-all(bf16[1,8,24,2048]{3,2,0,1:T(8,128)(2,1)S(1)} %bitcast.98), channel_id=1, replica_groups=mesh['ep'=8,'tp'=4] {'ep'}, dimensions={1} | all-to-all | bytes 1572864 | tf_op jit(solution)/shard_map/all_to_all | solution.py:154
  37.9 29.8 %all-gather.5.cloned.1.call-done = bf16[4,8,24,2048]{3,2,1,0:T(8,128)(2,1)} async-done(((bf16[1,8,24,2048]{3,2,1,0:T(8,128)(2,1)}), bf16[4,8,24,2048]{3,2,1,0:T(8,128)(2,1)}) %all-gather.5.cloned.1.call-update) | async-done | bytes 3145744 | tf_op jit(solution)/shard_map/all_gather | solution.py:153
  67.7 6.5 %fusion.13 = f32[4,8,24,896]{3,2,1,0:T(8,128)S(1)} fusion(bf16[4,8,24,2048]{3,2,1,0:T(8,128)(2,1)} %all-gather.5.cloned.1.call-done, bf16[1,2048,896]{2,1,0:T(8,128)(2,1)} %param.36), kind=kOutput, calls=%fused_computation.19 | convolution fusion | flops 2818572288 | bytes 9568256 | tf_op jit(solution)/shard_map/abcd,df->abcf/dot_general | solution.py:160
  74.3 3.7 %multiply_convert_fusion = bf16[4,8,24,896]{3,2,1,0:T(8,128)(2,1)S(1)} fusion(f32[4,8,24,896]{3,2,1,0:T(8,128)S(1)} %fusion.13, bf16[4,8,24,2048]{3,2,1,0:T(8,128)(2,1)S(1)} %copy-done.11, bf16[1,2048,896]{2,1,0:T(8,128)(2,1)S(1)} %copy-done.9), kind=kOutput, calls=%fused_computation.23 | convolution fusion | flops 2822701056 | bytes 10944512 | tf_op jit(solution)/shard_map/abcd,df->abcf/dot_general | solution.py:159
  78.1 5.3 %fusion.11 = f32[4,8,24,2048]{3,2,1,0:T(8,128)} fusion(bf16[4,8,24,896]{3,2,1,0:T(8,128)(2,1)S(1)} %multiply_convert_fusion, bf16[1,896,2048]{2,1,0:T(8,128)(2,1)S(1)} %copy-done.10), kind=kOutput, calls=%fused_computation.17 | convolution fusion | flops 2818572288 | bytes 11337728 | tf_op jit(solution)/shard_map/abcf,fd->abcd/dot_general | solution.py:163
  83.5 0.8 copy-done.1
  86.8 55.6 %reduce-scatter.2.cloned.1.call-done = f32[1,8,24,2048]{3,2,1,0:T(8,128)} async-done(((f32[4,8,24,2048]{3,2,1,0:T(8,128)}), f32[1,8,24,2048]{3,2,1,0:T(8,128)}) %reduce-scatter.2.cloned.1.call-update) | async-done | bytes 1572880 | tf_op jit(solution)/shard_map/reduce_scatter | solution.py:162
  142.4 2.4 %convert_bitcast_fusion = bf16[1,8,24,2048]{3,2,0,1:T(8,128)(2,1)} fusion(f32[1,8,24,2048]{3,2,1,0:T(8,128)} %reduce-scatter.2.cloned.1.call-done), kind=kLoop, calls=%fused_computation.29 | loop fusion | flops 393216 | bytes 2359296 | tf_op jit(solution)/shard_map/convert_element_type | solution.py:167
  144.8 6.0 %all-to-all-start.1 = ((bf16[1,8,24,2048]{3,2,0,1:T(8,128)(2,1)}), bf16[1,8,24,2048]{3,2,0,1:T(8,128)(2,1)S(1)}, u32[]{:S(2)}, u32[]{:S(2)}) async-start(bf16[1,8,24,2048]{3,2,0,1:T(8,128)(2,1)} %convert_bitcast_fusion), calls=%async_computation.2 | async-start | bytes 1572864 | tf_op jit(solution)/shard_map/all_to_all | solution.py:168
  151.1 38.3 %all_gather.10 = bf16[2048,64]{0,1:T(8,128)(2,1)S(1)} all-gather(bf16[256,64]{0,1:T(8,128)(2,1)S(1)} %pad_maximum_fusion.2), channel_id=1, replica_groups=mesh['ep'=8,'tp'=4] {'ep'}, dimensions={0}, use_global_device_ids=true | all-gather | bytes 294912 | tf_op jit(solution)/shard_map/all_gather | solution.py:81
  189.4 16.3 %while.13 = (s32[]{:T(128)}, f32[256,2,128]{2,0,1:T(8,128)S(1)}, f32[2,256]{1,0:T(2,128)S(1)}, s32[4]{0:T(128)S(1)}, s32[]{:T(128)}, /*index=5*/bf16[2048,512]{0...) while((s32[]{:T(128)}, f32[256,2,128]{2,0,1:T(8,128)S(1)}, ...), condition=%wide.region_8.9_spmd.clone, body=%wide.region_4.8_spmd.clone.sunk | while | flops 169280256 | bytes 5783885 | solution.py:123
  190.6 2.8 %conditional.3 = ((f32[256,2,128]{2,0,1:T(8,128)S(1)}, f32[2,256]{1,0:T(2,128)S(1)})) conditional(s32[]{:T(128)} %convert_element_type.127, (f32[256,2,128]{2,0,1:T(8,128)S(1)}, f32[2,256]{1,0:T(2,128)S(1)}) %tuple.58, (s32[]{:T(128)}, s32[]{:T(128)}, bf16[2048,512]{0,1:T(8,128)(2,1)}, bf16[256,2,128]{2,0,1:T(8,128)(2,1)S(1)}, ...), branch_computations={%region_5.5_spmd, %region_6.7_spmd} | conditional | flops 169280256 | bytes 5782618 | solution.py:121
  190.7 1.3 constant_dynamic-slice_fusion
  194.7 2.8 %conditional.3 = ((f32[256,2,128]{2,0,1:T(8,128)S(1)}, f32[2,256]{1,0:T(2,128)S(1)})) conditional(s32[]{:T(128)} %convert_element_type.127, (f32[256,2,128]{2,0,1:T(8,128)S(1)}, f32[2,256]{1,0:T(2,128)S(1)}) %tuple.58, (s32[]{:T(128)}, s32[]{:T(128)}, bf16[2048,512]{0,1:T(8,128)(2,1)}, bf16[256,2,128]{2,0,1:T(8,128)(2,1)S(1)}, ...), branch_computations={%region_5.5_spmd, %region_6.7_spmd} | conditional | flops 169280256 | bytes 5782618 | solution.py:121
  194.8 1.3 constant_dynamic-slice_fusion
  198.8 2.8 %conditional.3 = ((f32[256,2,128]{2,0,1:T(8,128)S(1)}, f32[2,256]{1,0:T(2,128)S(1)})) conditional(s32[]{:T(128)} %convert_element_type.127, (f32[256,2,128]{2,0,1:T(8,128)S(1)}, f32[2,256]{1,0:T(2,128)S(1)}) %tuple.58, (s32[]{:T(128)}, s32[]{:T(128)}, bf16[2048,512]{0,1:T(8,128)(2,1)}, bf16[256,2,128]{2,0,1:T(8,128)(2,1)S(1)}, ...), branch_computations={%region_5.5_spmd, %region_6.7_spmd} | conditional | flops 169280256 | bytes 5782618 | solution.py:121
  198.8 1.3 constant_dynamic-slice_fusion
  202.9 2.7 %conditional.3 = ((f32[256,2,128]{2,0,1:T(8,128)S(1)}, f32[2,256]{1,0:T(2,128)S(1)})) conditional(s32[]{:T(128)} %convert_element_type.127, (f32[256,2,128]{2,0,1:T(8,128)S(1)}, f32[2,256]{1,0:T(2,128)S(1)}) %tuple.58, (s32[]{:T(128)}, s32[]{:T(128)}, bf16[2048,512]{0,1:T(8,128)(2,1)}, bf16[256,2,128]{2,0,1:T(8,128)(2,1)S(1)}, ...), branch_computations={%region_5.5_spmd, %region_6.7_spmd} | conditional | flops 169280256 | bytes 5782618 | solution.py:121
  202.9 1.3 constant_dynamic-slice_fusion
  205.9 0.9 copy_bitcast_fusion
  206.8 1.0 fusion.19
  (117 shorter events, 13.5 us)
Async XLA Ops:
  8.0 76.5 %copy-start = (bf16[512,256]{1,0:T(8,128)(2,1)S(1)}, bf16[512,256]{1,0:T(8,128)(2,1)}, u32[]{:S(2)}) copy-start(bf16[512,256]{1,0:T(8,128)(2,1)} %param.25) | copy-start | bytes 786436
  8.0 59.7 %all-gather.5.cloned.1.call-start = ((), (), s32[]{:S(2)}) async-start(), calls=%async_computation.4 | async-start | bytes 3932160 | tf_op jit(solution)/shard_map/all_gather | solution.py:153
  9.6 4.4 %copy-start.4 = (f32[2048]{0:T(1024)S(1)}, f32[2048]{0:T(1024)}, u32[]{:S(2)}) copy-start(f32[2048]{0:T(1024)} %param.32) | copy-start | bytes 24580
  37.8 104.5 %reduce-scatter.2.cloned.1.call-start = ((), (), s32[]{:S(2)}) async-start(), calls=%async_computation.5 | async-start | bytes 7864320 | tf_op jit(solution)/shard_map/reduce_scatter | solution.py:162
  67.7 6.6 %copy-start.9 = (bf16[1,2048,896]{2,1,0:T(8,128)(2,1)S(1)}, bf16[1,2048,896]{2,1,0:T(8,128)(2,1)}, u32[]{:S(2)}) copy-start(bf16[1,2048,896]{2,1,0:T(8,128)(2,1)} %param.35) | copy-start | bytes 11010052
  67.7 6.6 %copy-start.11 = (bf16[4,8,24,2048]{3,2,1,0:T(8,128)(2,1)S(1)}, bf16[4,8,24,2048]{3,2,1,0:T(8,128)(2,1)}, u32[]{:S(2)}) copy-start(bf16[4,8,24,2048]{3,2,1,0:T(8,128)(2,1)} %all-gather.5.cloned.1.call-done) | copy-start | bytes 9437188
  74.3 3.8 %copy-start.10 = (bf16[1,896,2048]{2,1,0:T(8,128)(2,1)S(1)}, bf16[1,896,2048]{2,1,0:T(8,128)(2,1)}, u32[]{:S(2)}) copy-start(bf16[1,896,2048]{2,1,0:T(8,128)(2,1)} %param.37) | copy-start | bytes 11010052
  83.4 0.9 copy-start.1
  83.4 1.1 copy-start.14
  83.4 1.1 copy-start.13
  83.4 1.6 copy-start.12
  83.4 2.7 %copy-start.2 = (bf16[256,384]{1,0:T(8,128)(2,1)S(1)}, bf16[256,384]{1,0:T(8,128)(2,1)}, u32[]{:S(2)}) copy-start(bf16[256,384]{1,0:T(8,128)(2,1)} %param.21) | copy-start | bytes 589828
  83.4 2.9 %copy-start.5 = (f32[192]{0:T(256)S(1)}, f32[192]{0:T(256)}, u32[]{:S(2)}) copy-start(f32[192]{0:T(256)} %param.27) | copy-start | bytes 2308
  83.4 3.2 %copy-start.8 = (f32[256,2]{0,1:T(2,128)S(1)}, f32[256,2]{0,1:T(2,128)}, u32[]{:S(2)}) copy-start(f32[256,2]{0,1:T(2,128)} %param.34) | copy-start | bytes 6148
  83.4 3.3 %copy-start.3 = (bf16[256,64]{0,1:T(8,128)(2,1)S(1)}, bf16[256,64]{0,1:T(8,128)(2,1)}, u32[]{:S(2)}) copy-start(bf16[256,64]{0,1:T(8,128)(2,1)} %param.23) | copy-start | bytes 98308
  83.4 3.3 %copy-start.6 = (f32[64]{0:T(128)S(1)}, f32[64]{0:T(128)}, u32[]{:S(2)}) copy-start(f32[64]{0:T(128)} %param.29) | copy-start | bytes 772
  83.4 105.9 %all-gather.3.cloned.1.call-start = ((), (), s32[]{:S(2)}) async-start(), calls=%async_computation.3 | async-start | bytes 2359296 | tf_op jit(solution)/shard_map/all_gather | solution.py:80
  144.8 62.0 %all-to-all-start.1 = ((bf16[1,8,24,2048]{3,2,0,1:T(8,128)(2,1)}), bf16[1,8,24,2048]{3,2,0,1:T(8,128)(2,1)S(1)}, u32[]{:S(2)}, u32[]{:S(2)}) async-start(bf16[1,8,24,2048]{3,2,0,1:T(8,128)(2,1)} %convert_bitcast_fusion), calls=%async_computation.2 | async-start | bytes 1572864 | tf_op jit(solution)/shard_map/all_to_all | solution.py:168
  189.4 16.5 %copy-start.7 = (f32[128]{0:T(128)S(1)}, f32[128]{0:T(128)}, u32[]{:S(2)}) copy-start(f32[128]{0:T(128)} %param.30) | copy-start | bytes 1540
Sparse Core Ops, SparseCore 0:
  38.0 29.6 all-gather.4
  83.5 58.8 reduce-scatter.1
Sparse Core Ops, SparseCore 1:
  86.5 48.5 all-gather.2
where the time goes:
time: 216 us; the launch traced here: 215 us
  waiting for transfers between devices  85.4 us (40%)
  blocking collectives  61.7 us (29%)
  matrix products  22.6 us (10%)
  between operations  15.9 us (7%)
  local copies, waits for them, and re-layouts  10.3 us (5%)
  other arithmetic  10.1 us (5%)
  starting transfers between devices  6.13 us (3%)
  loops' own time  3.02 us (1%)
    reduce_scatter x1, waiting for transfers between devices, experts_part(): lax.psum_scatter(jnp.einsum('abcf,fd->abcd', hidden, down_cols, preferred...  55.6 us
    all_gather x1, blocking collectives, attention_part(): rope_piece = lax.all_gather(rot_key, 'ep', axis=0, tiled=True)  38.3 us
    all_gather x1, waiting for transfers between devices, experts_part(): lax.all_gather(lax.all_to_all(outgoing, 'ep', split_axis=1, concat_axis=1...  29.8 us
    all_to_all x1, blocking collectives, experts_part(): lax.all_to_all(outgoing, 'ep', split_axis=1, concat_axis=1, tiled=True)  23.4 us
    dot_general x1, matrix products, experts_part(): jnp.einsum('abcd,df->abcf', arrived, w_up[0], preferred_element_type=jnp....  6.55 us
    all_to_all x1, starting transfers between devices, experts_part(): lax.all_to_all(summed, 'ep', split_axis=1, concat_axis=1, tiled=True)  6.01 us
    slice x4, local copies, waits for them, and re-layouts, attend(): kv_block[:, :head_count * nope_dim]  5.31 us
    dot_general x1, matrix products, experts_part(): jnp.einsum('abcf,fd->abcd', hidden, down_cols, preferred_element_type=jnp...  5.3 us
  transfers between devices with their start and end apart: 4, of which 2 were waited for; matrix products, arithmetic and copies ran while one was open for 9% of the time, Pallas kernels for 0%

commit v1 on v0

--- a/solution.py
+++ b/solution.py
@@ -77,8 +77,11 @@
         jnp.zeros((head_count, tok_rows), jnp.float32),
     )
     totals = initial
-    key_piece = lax.all_gather(keys_values, "ep", axis=0, tiled=True)
-    rope_piece = lax.all_gather(rot_key, "ep", axis=0, tiled=True)
+    key_piece, rope_piece = jnp.split(
+        lax.all_gather(jnp.concatenate([keys_values, rot_key], axis=1), "ep", axis=0, tiled=True),
+        [keys_values.shape[1]],
+        axis=1,
+    )
     piece_rows = key_piece.shape[0]
     block_rows = math.gcd(piece_rows, 512)
 

time: 216 us -> 185 us (0.86)
  blocking collectives: 61.7 us -> 23.4 us
  matrix products: 22.6 us -> 27.1 us
  local copies, waits for them, and re-layouts: 10.3 us -> 12.5 us
    all_gather x1 -> x0, blocking collectives: 38.3 us -> none  [attention_part(): rope_piece = lax.all_gather(rot_key, 'ep', axis=0, tiled=True)]
    slice x4, local copies, waits for them, and re-layouts: 5.31 us -> 1.07 us  [attend(): kv_block[:, :head_count * nope_dim]]
    dot_general x4, matrix products: 2.13 us -> 5.67 us  [attend(): jnp.einsum('qhr,kr->hqk', query_rope, rope_block, preferred_element_type=...]
    split x0 -> x2, local copies, waits for them, and re-layouts: none -> 3.4 us  [attention_part(): jnp.split(lax.all_gather(jnp.concatenate([keys_values, rot_key], axis=1),...]
    dynamic_slice x4, local copies, waits for them, and re-layouts: 2.35 us -> 4.85 us  [attention_part(): lax.scan(one_block, totals, jnp.arange(piece_rows // block_rows, dtype=jn...]
  transfers between devices with their start and end apart: 4 -> 4, of which waited for: 2 -> 2; matrix products, arithmetic and copies ran while one was open for 9% -> 14% of each run, Pallas kernels for 0% -> 0%
where the time goes in v1:
time: 185 us; the launch traced here: 184 us
  waiting for transfers between devices  85.6 us (46%)
  matrix products  27.1 us (15%)
  blocking collectives  23.4 us (13%)
  between operations  15.9 us (9%)
  local copies, waits for them, and re-layouts  12.5 us (7%)
  other arithmetic  10.8 us (6%)
  starting transfers between devices  6.13 us (3%)
  loops' own time  2.98 us (2%)
    reduce_scatter x1, waiting for transfers between devices, experts_part(): lax.psum_scatter(jnp.einsum('abcf,fd->abcd', hidden, down_cols, preferred...  55.7 us
    all_gather x1, waiting for transfers between devices, experts_part(): lax.all_gather(lax.all_to_all(outgoing, 'ep', split_axis=1, concat_axis=1...  29.8 us
    all_to_all x1, blocking collectives, experts_part(): lax.all_to_all(outgoing, 'ep', split_axis=1, concat_axis=1, tiled=True)  23.4 us
    dot_general x1, matrix products, experts_part(): jnp.einsum('abcd,df->abcf', arrived, w_up[0], preferred_element_type=jnp....  6.54 us
    all_to_all x1, starting transfers between devices, experts_part(): lax.all_to_all(summed, 'ep', split_axis=1, concat_axis=1, tiled=True)  6.01 us
    dot_general x4, matrix products, attend(): jnp.einsum('qhr,kr->hqk', query_rope, rope_block, preferred_element_type=...  5.67 us
    dot_general x1, matrix products, experts_part(): jnp.einsum('abcf,fd->abcd', hidden, down_cols, preferred_element_type=jnp...  5.41 us
    dynamic_slice x4, local copies, waits for them, and re-layouts, attention_part(): lax.scan(one_block, totals, jnp.arange(piece_rows // block_rows, dtype=jn...  4.85 us
  transfers between devices with their start and end apart: 4, of which 2 were waited for; matrix products, arithmetic and copies ran while one was open for 14% of the time, Pallas kernels for 0%

profile of v1, /device:TPU:24, one launch (start us, length us, event | category | flops | bytes accessed | tf_op | source)
XLA Modules:
  0.0 184.4 jit_solution(3810334742739892177)
XLA Ops:
  9.6 1.5 multiply_reduce_fusion
  11.1 1.5 convert_element_type.75
  14.4 23.4 %all_to_all.10 = bf16[1,8,24,2048]{3,2,0,1:T(8,128)(2,1)} all-to-all(bf16[1,8,24,2048]{3,2,0,1:T(8,128)(2,1)S(1)} %bitcast.98), channel_id=1, replica_groups=mesh['ep'=8,'tp'=4] {'ep'}, dimensions={1} | all-to-all | bytes 1572864 | tf_op jit(solution)/shard_map/all_to_all | solution.py:157
  37.9 29.8 %all-gather.5.cloned.1.call-done = bf16[4,8,24,2048]{3,2,1,0:T(8,128)(2,1)} async-done(((bf16[1,8,24,2048]{3,2,1,0:T(8,128)(2,1)}), bf16[4,8,24,2048]{3,2,1,0:T(8,128)(2,1)}) %all-gather.5.cloned.1.call-update) | async-done | bytes 3145744 | tf_op jit(solution)/shard_map/all_gather | solution.py:156
  67.7 6.5 %fusion.13 = f32[4,8,24,896]{3,2,1,0:T(8,128)S(1)} fusion(bf16[4,8,24,2048]{3,2,1,0:T(8,128)(2,1)} %all-gather.5.cloned.1.call-done, bf16[1,2048,896]{2,1,0:T(8,128)(2,1)} %param.36), kind=kOutput, calls=%fused_computation.19 | convolution fusion | flops 2818572288 | bytes 9568256 | tf_op jit(solution)/shard_map/abcd,df->abcf/dot_general | solution.py:163
  74.3 3.7 %multiply_convert_fusion = bf16[4,8,24,896]{3,2,1,0:T(8,128)(2,1)S(1)} fusion(f32[4,8,24,896]{3,2,1,0:T(8,128)S(1)} %fusion.13, bf16[4,8,24,2048]{3,2,1,0:T(8,128)(2,1)S(1)} %copy-done.12, bf16[1,2048,896]{2,1,0:T(8,128)(2,1)S(1)} %copy-done.10), kind=kOutput, calls=%fused_computation.23 | convolution fusion | flops 2822701056 | bytes 10944512 | tf_op jit(solution)/shard_map/abcd,df->abcf/dot_general | solution.py:162
  78.1 5.4 %fusion.11 = f32[4,8,24,2048]{3,2,1,0:T(8,128)} fusion(bf16[4,8,24,896]{3,2,1,0:T(8,128)(2,1)S(1)} %multiply_convert_fusion, bf16[1,896,2048]{2,1,0:T(8,128)(2,1)S(1)} %copy-done.11), kind=kOutput, calls=%fused_computation.17 | convolution fusion | flops 2818572288 | bytes 11337728 | tf_op jit(solution)/shard_map/abcf,fd->abcd/dot_general | solution.py:166
  86.8 55.7 %reduce-scatter.2.cloned.1.call-done = f32[1,8,24,2048]{3,2,1,0:T(8,128)} async-done(((f32[4,8,24,2048]{3,2,1,0:T(8,128)}), f32[1,8,24,2048]{3,2,1,0:T(8,128)}) %reduce-scatter.2.cloned.1.call-update) | async-done | bytes 1572880 | tf_op jit(solution)/shard_map/reduce_scatter | solution.py:165
  142.5 2.4 %convert_bitcast_fusion = bf16[1,8,24,2048]{3,2,0,1:T(8,128)(2,1)} fusion(f32[1,8,24,2048]{3,2,1,0:T(8,128)} %reduce-scatter.2.cloned.1.call-done), kind=kLoop, calls=%fused_computation.29 | loop fusion | flops 393216 | bytes 2359296 | tf_op jit(solution)/shard_map/convert_element_type | solution.py:170
  144.9 6.0 %all-to-all-start.1 = ((bf16[1,8,24,2048]{3,2,0,1:T(8,128)(2,1)}), bf16[1,8,24,2048]{3,2,0,1:T(8,128)(2,1)S(1)}, u32[]{:S(2)}, u32[]{:S(2)}) async-start(bf16[1,8,24,2048]{3,2,0,1:T(8,128)(2,1)} %convert_bitcast_fusion), calls=%async_computation.2 | async-start | bytes 1572864 | tf_op jit(solution)/shard_map/all_to_all | solution.py:171
  152.0 1.7 split.8
  153.7 1.7 split.9
  155.9 18.0 %while.13 = (s32[]{:T(128)}, f32[256,2,128]{2,0,1:T(8,128)S(1)}, f32[2,256]{1,0:T(2,128)S(1)}, s32[4]{0:T(128)}, s32[]{:T(128)}, /*index=5*/bf16[2048,512]{0,1:T...) while((s32[]{:T(128)}, f32[256,2,128]{2,0,1:T(8,128)S(1)}, ...), condition=%wide.region_8.9_spmd.clone, body=%wide.region_4.8_spmd.clone.sunk | while | flops 169280256 | bytes 5783885 | solution.py:126
  156.0 1.2 dynamic_slice.62
  157.8 2.6 %conditional.3 = ((f32[256,2,128]{2,0,1:T(8,128)S(1)}, f32[2,256]{1,0:T(2,128)S(1)})) conditional(s32[]{:T(128)} %convert_element_type.127, (f32[256,2,128]{2,0,1:T(8,128)S(1)}, f32[2,256]{1,0:T(2,128)S(1)}) %tuple.58, (s32[]{:T(128)}, s32[]{:T(128)}, bf16[2048,512]{0,1:T(8,128)(2,1)S(1)}, bf16[256,2,128]{2,0,1:T(8,128)(2,1)S(1)}, ...), branch_computations={%region_5.5_spmd, %region_6.7_spmd} | conditional | flops 169280256 | bytes 5782618 | solution.py:124
  158.6 1.4 fusion.42
  160.5 1.2 dynamic_slice.62
  162.3 2.6 %conditional.3 = ((f32[256,2,128]{2,0,1:T(8,128)S(1)}, f32[2,256]{1,0:T(2,128)S(1)})) conditional(s32[]{:T(128)} %convert_element_type.127, (f32[256,2,128]{2,0,1:T(8,128)S(1)}, f32[2,256]{1,0:T(2,128)S(1)}) %tuple.58, (s32[]{:T(128)}, s32[]{:T(128)}, bf16[2048,512]{0,1:T(8,128)(2,1)S(1)}, bf16[256,2,128]{2,0,1:T(8,128)(2,1)S(1)}, ...), branch_computations={%region_5.5_spmd, %region_6.7_spmd} | conditional | flops 169280256 | bytes 5782618 | solution.py:124
  163.2 1.4 fusion.42
  166.9 2.6 %conditional.3 = ((f32[256,2,128]{2,0,1:T(8,128)S(1)}, f32[2,256]{1,0:T(2,128)S(1)})) conditional(s32[]{:T(128)} %convert_element_type.127, (f32[256,2,128]{2,0,1:T(8,128)S(1)}, f32[2,256]{1,0:T(2,128)S(1)}) %tuple.58, (s32[]{:T(128)}, s32[]{:T(128)}, bf16[2048,512]{0,1:T(8,128)(2,1)S(1)}, bf16[256,2,128]{2,0,1:T(8,128)(2,1)S(1)}, ...), branch_computations={%region_5.5_spmd, %region_6.7_spmd} | conditional | flops 169280256 | bytes 5782618 | solution.py:124
  167.7 1.4 fusion.42
  171.4 2.6 %conditional.3 = ((f32[256,2,128]{2,0,1:T(8,128)S(1)}, f32[2,256]{1,0:T(2,128)S(1)})) conditional(s32[]{:T(128)} %convert_element_type.127, (f32[256,2,128]{2,0,1:T(8,128)S(1)}, f32[2,256]{1,0:T(2,128)S(1)}) %tuple.58, (s32[]{:T(128)}, s32[]{:T(128)}, bf16[2048,512]{0,1:T(8,128)(2,1)S(1)}, bf16[256,2,128]{2,0,1:T(8,128)(2,1)S(1)}, ...), branch_computations={%region_5.5_spmd, %region_6.7_spmd} | conditional | flops 169280256 | bytes 5782618 | solution.py:124
  172.2 1.4 fusion.42
  175.1 1.8 fusion.19
  (119 shorter events, 16.2 us)
Async XLA Ops:
  8.0 76.6 %copy-start = (bf16[512,256]{1,0:T(8,128)(2,1)S(1)}, bf16[512,256]{1,0:T(8,128)(2,1)}, u32[]{:S(2)}) copy-start(bf16[512,256]{1,0:T(8,128)(2,1)} %param.25) | copy-start | bytes 786436
  8.0 59.7 %all-gather.5.cloned.1.call-start = ((), (), s32[]{:S(2)}) async-start(), calls=%async_computation.4 | async-start | bytes 3932160 | tf_op jit(solution)/shard_map/all_gather | solution.py:156
  9.6 4.4 %copy-start.5 = (f32[2048]{0:T(1024)S(1)}, f32[2048]{0:T(1024)}, u32[]{:S(2)}) copy-start(f32[2048]{0:T(1024)} %param.32) | copy-start | bytes 24580
  13.9 60.4 %copy-start.2 = (pred[4,64,2,192]{3,1,2,0:T(32,128)(4,1)}, pred[4,64,2,192]{3,1,2,0:T(32,128)(4,1)S(1)}, u32[]{:S(2)}) copy-start(pred[4,64,2,192]{3,1,2,0:T(32,128)(4,1)S(1)} %iota_compare_fusion) | copy-start | bytes 294916
  37.9 104.7 %reduce-scatter.2.cloned.1.call-start = ((), (), s32[]{:S(2)}) async-start(), calls=%async_computation.5 | async-start | bytes 7864320 | tf_op jit(solution)/shard_map/reduce_scatter | solution.py:165
  67.7 6.6 %copy-start.10 = (bf16[1,2048,896]{2,1,0:T(8,128)(2,1)S(1)}, bf16[1,2048,896]{2,1,0:T(8,128)(2,1)}, u32[]{:S(2)}) copy-start(bf16[1,2048,896]{2,1,0:T(8,128)(2,1)} %param.35) | copy-start | bytes 11010052
  67.7 6.6 %copy-start.12 = (bf16[4,8,24,2048]{3,2,1,0:T(8,128)(2,1)S(1)}, bf16[4,8,24,2048]{3,2,1,0:T(8,128)(2,1)}, u32[]{:S(2)}) copy-start(bf16[4,8,24,2048]{3,2,1,0:T(8,128)(2,1)} %all-gather.5.cloned.1.call-done) | copy-start | bytes 9437188
  74.3 3.7 %copy-start.11 = (bf16[1,896,2048]{2,1,0:T(8,128)(2,1)S(1)}, bf16[1,896,2048]{2,1,0:T(8,128)(2,1)}, u32[]{:S(2)}) copy-start(bf16[1,896,2048]{2,1,0:T(8,128)(2,1)} %param.37) | copy-start | bytes 11010052
  83.5 0.9 copy-start.1
  83.5 1.1 copy-start.15
  83.5 1.1 copy-start.14
  83.5 1.7 copy-start.4
  83.5 1.7 copy-start.7
  83.5 2.0 %copy-start.13 = (bf16[512,256]{1,0:T(8,128)(2,1)S(1)}, bf16[512,256]{1,0:T(8,128)(2,1)}, u32[]{:S(2)}) copy-start(bf16[512,256]{1,0:T(8,128)(2,1)} %param.26) | copy-start | bytes 786436
  83.5 3.1 %copy-start.3 = (bf16[256,384]{1,0:T(8,128)(2,1)S(1)}, bf16[256,384]{1,0:T(8,128)(2,1)}, u32[]{:S(2)}) copy-start(bf16[256,384]{1,0:T(8,128)(2,1)} %param.21) | copy-start | bytes 589828
  83.5 68.4 %all-gather.3.cloned.1.call-start = ((), (), s32[]{:S(2)}) async-start(), calls=%async_computation.3 | async-start | bytes 2654208 | tf_op jit(solution)/shard_map/all_gather | solution.py:81
  86.6 64.4 %copy-start.6 = (f32[192]{0:T(256)S(1)}, f32[192]{0:T(256)}, u32[]{:S(2)}) copy-start(f32[192]{0:T(256)} %param.27) | copy-start | bytes 2308
  86.7 64.5 %copy-start.9 = (f32[256,2]{0,1:T(2,128)S(1)}, f32[256,2]{0,1:T(2,128)}, u32[]{:S(2)}) copy-start(f32[256,2]{0,1:T(2,128)} %param.34) | copy-start | bytes 6148
  144.9 30.2 %all-to-all-start.1 = ((bf16[1,8,24,2048]{3,2,0,1:T(8,128)(2,1)}), bf16[1,8,24,2048]{3,2,0,1:T(8,128)(2,1)S(1)}, u32[]{:S(2)}, u32[]{:S(2)}) async-start(bf16[1,8,24,2048]{3,2,0,1:T(8,128)(2,1)} %convert_bitcast_fusion), calls=%async_computation.2 | async-start | bytes 1572864 | tf_op jit(solution)/shard_map/all_to_all | solution.py:171
  155.9 18.3 %copy-start.8 = (f32[128]{0:T(128)S(1)}, f32[128]{0:T(128)}, u32[]{:S(2)}) copy-start(f32[128]{0:T(128)} %param.30) | copy-start | bytes 1540
Sparse Core Ops, SparseCore 0:
  38.0 29.6 all-gather.4
  83.6 58.8 reduce-scatter.1
Sparse Core Ops, SparseCore 1:
  86.7 51.4 all-gather.2
